TPU v7x, 512 devices: a whole 4x4x16 slice. The times are simulated.
512 devices in a mesh: sp: 32 (over z, core), tp: 16 (over y, x).
Axes of the slice: x: 4, y: 4, z: 16, core: 2. Of those that a mesh axis runs over, the one named last changes fastest.
Arguments:
- query_proj: bfloat16 [8192, 2048], P('sp', 'tp'), may hold values from -4 to 4
- key_proj: bfloat16 [8192, 1024], P('sp', 'tp'), may hold values from -4 to 4
- value_proj: bfloat16 [8192, 1024], P('sp', 'tp'), may hold values from -48 to 48
- query_gain: float32 [32, 64], P('tp'), may hold values from 1 to 6
- key_gain: float32 [16, 64], P('tp'), may hold values from 1 to 6
- residual: bfloat16 [8192, 2048], P('sp', 'tp'), may hold values from -48 to 48
- out_weight: bfloat16 [2048, 2048], P(None, 'tp'), may hold values from -0.125 to 0.125
- route_expert: int32 [8192, 8], P('sp'), may hold values from 0 to 255, all different within a row; in each aligned block of 256 rows (0 to 255, 256 to 511, ...) at most 12 rows name the same one
- route_weight: float32 [8192, 8], P('sp'), may hold values from 0.25 to 1.25
- expert_gate: bfloat16 [512, 2048, 256], P(('sp', 'tp')), may hold values from -0.125 to 0.125
- expert_up: bfloat16 [512, 2048, 256], P(('sp', 'tp')), may hold values from -0.125 to 0.125
- expert_down: bfloat16 [512, 256, 2048], P(('sp', 'tp')), may hold values from -0.25 to 0.25
Outputs:
- block_out: bfloat16 [8192, 2048], P('sp', 'tp')
Inputs may be any that keep to these rules, and one draw needn't show every extreme that they name: `route_expert`: A row names 8 different experts; among the rows of one index of sp no expert is named by more than 12 rows, a bound that some block reaches of them.
All inputs are finite; a program needn't handle non-finite values.
Results may differ from a plain program's by a relative error of at most 0.012.
The roundings to bfloat16 on the way count: a program that leaves them out, or rounds other values in their place, can miss the bound.
Values may be sent and summed in bfloat16 or wider, within the bound.
A program may use at most 64 MiB of HBM per device.

v0:
```python
import math
import jax
import jax.numpy as jnp
from jax import lax
from jax.sharding import Mesh
from jax.sharding import PartitionSpec as P

HEAD_DIM = 64
TOP_K = 8
GRID_W = 64
SP = ("sp_0", "sp_1")
SP_TP = ("sp_0", "sp_1", "tp")
EPSILON = 1e-06
ROPE_BASE = 10000.0
KEY_BLOCK = 1024


def laid_out(pieces, dim):
    shape = list(pieces.shape[1:])
    shape[dim] *= pieces.shape[0]
    return jnp.moveaxis(pieces, 0, dim).reshape(shape)


def from_everyone(x, axis):
    devices = lax.axis_size(axis)
    return lax.all_to_all(jnp.broadcast_to(x[None], (devices, *x.shape)), axis, 0, 0, tiled=True)


def gather_directly(x, axis, dim):
    return laid_out(from_everyone(x, axis), dim)


def cut_along(x, dim, devices):
    shape = x.shape
    pieces = x.reshape(*shape[:dim], devices, shape[dim] // devices, *shape[dim + 1 :])
    return jnp.moveaxis(pieces, dim, 0)


def turned_blocks(pieces, axes, sequence):
    shape = [lax.axis_size(a) for a in axes]
    pieces = pieces.reshape(*shape, *pieces.shape[1:])
    for k in sequence:
        pieces = lax.all_to_all(pieces, axes[k], split_axis=k, concat_axis=k, tiled=True)
    return pieces.reshape(-1, *pieces.shape[len(axes) :])


def core_and_chips(x, groups, sequence, split_dim, concat_dim):
    devices = lax.axis_size(groups[0]) * lax.axis_size(groups[1])
    pieces = cut_along(x, split_dim, devices)
    return laid_out(turned_blocks(pieces, groups, sequence), concat_dim)


def swapped(value, axis, stride):
    mask = 2**stride
    pairs = [(source, source ^ mask) for source in range(lax.axis_size(axis))]
    return lax.ppermute(value, axis, pairs)


def summed_on_arrival(x, axis, dim):
    devices = lax.axis_size(axis)
    pieces = lax.all_to_all(cut_along(x, dim, devices), axis, 0, 0, tiled=True)
    return jnp.sum(pieces.astype(jnp.float32), axis=0)


def rotation_tables(offset, count):
    pair_count = HEAD_DIM // 4
    position = offset + jnp.arange(count, dtype=jnp.int32)
    grid_row = (position // GRID_W).astype(jnp.float32)
    grid_col = (position % GRID_W).astype(jnp.float32)
    inverse = ROPE_BASE ** (-jnp.arange(pair_count, dtype=jnp.float32) / pair_count)
    angles = jnp.stack([grid_row[:, None] * inverse, grid_col[:, None] * inverse], axis=1)
    return (jnp.cos(angles), jnp.sin(angles))


def rotate(vectors, cosine_table, sine_table):
    pair_count = HEAD_DIM // 4
    shaped = vectors.reshape(vectors.shape[:-1] + (2, 2, pair_count))
    first_half = shaped[..., 0, :]
    second_half = shaped[..., 1, :]
    cosine_row = cosine_table[:, None]
    sine_row = sine_table[:, None]
    turned = jnp.stack(
        [
            first_half * cosine_row - second_half * sine_row,
            first_half * sine_row + second_half * cosine_row,
        ],
        axis=-2,
    )
    return turned.reshape(vectors.shape)


def head_norm(vectors, gain):
    scaled = vectors.astype(jnp.float32)
    scaled = scaled * lax.rsqrt(jnp.mean(scaled * scaled, axis=-1, keepdims=True) + EPSILON)
    return scaled * gain


def online_update(running, query_groups, key_block, value_block):
    running_max, running_sum, running_acc = running
    scores = jnp.einsum(
        "tkgd,nkd->kgtn", query_groups, key_block, preferred_element_type=jnp.float32
    ) * HEAD_DIM ** (-0.5)
    new_max = jnp.maximum(running_max, jnp.max(scores, axis=-1))
    rescale = jnp.exp(running_max - new_max)
    weights = jnp.exp(scores - new_max[..., None]).astype(jnp.bfloat16)
    new_sum = running_sum * rescale + jnp.sum(weights.astype(jnp.float32), axis=-1)
    update = jnp.einsum("kgtn,nkd->kgtd", weights, value_block, preferred_element_type=jnp.float32)
    return (new_max, new_sum, running_acc * rescale[..., None] + update)


def local(
    query_proj,
    key_proj,
    value_proj,
    query_gain,
    key_gain,
    residual,
    out_weight,
    route_expert,
    route_weight,
    expert_gate,
    expert_up,
    expert_down,
):
    token_count = query_proj.shape[0]
    local_heads = query_gain.shape[0]
    local_kv = key_gain.shape[0]
    group_size = local_heads // local_kv
    sp_size = lax.axis_size(SP)
    tp_size = lax.axis_size("tp")
    tp_place = lax.axis_index("tp")
    offset = lax.axis_index(SP) * token_count
    cosine_table, sine_table = rotation_tables(offset, token_count)
    query_rot = rotate(
        head_norm(query_proj.reshape(token_count, local_heads, HEAD_DIM), query_gain),
        cosine_table,
        sine_table,
    ).astype(jnp.bfloat16)
    key_rot = rotate(
        head_norm(key_proj.reshape(token_count, local_kv, HEAD_DIM), key_gain),
        cosine_table,
        sine_table,
    ).astype(jnp.bfloat16)
    packed = jnp.concatenate(
        [key_rot.reshape(token_count, local_kv * HEAD_DIM), value_proj], axis=1
    )
    query_groups = query_rot.reshape(token_count, local_kv, group_size, HEAD_DIM)
    initial = (
        jnp.full((local_kv, group_size, token_count), -1e30, jnp.float32),
        jnp.zeros((local_kv, group_size, token_count), jnp.float32),
        jnp.zeros((local_kv, group_size, token_count, HEAD_DIM), jnp.float32),
    )
    incoming = lax.all_gather(packed, SP, axis=0, tiled=True)
    incoming_len = incoming.shape[0]
    step_len = math.gcd(incoming_len, KEY_BLOCK)

    def one_step(step_index, running):
        block_rows = lax.dynamic_slice_in_dim(incoming, step_index * step_len, step_len, 0)
        key_block = block_rows[:, : local_kv * HEAD_DIM].reshape(step_len, local_kv, HEAD_DIM)
        value_block = block_rows[:, local_kv * HEAD_DIM :].reshape(step_len, local_kv, HEAD_DIM)
        return online_update(running, query_groups, key_block, value_block)

    final_max, final_sum, final_acc = lax.fori_loop(0, incoming_len // step_len, one_step, initial)
    attended = final_acc / final_sum[..., None]
    attended = jnp.transpose(attended, (2, 0, 1, 3)).reshape(token_count, local_heads * HEAD_DIM)
    attended = attended.astype(jnp.bfloat16)
    projected = jnp.dot(
        gather_directly(attended, "tp", 1), out_weight, preferred_element_type=jnp.float32
    )
    mixed_sum = residual.astype(jnp.float32) + projected
    mixed_rows = mixed_sum.astype(jnp.bfloat16)
    full_rows = gather_directly(mixed_rows, "tp", 1)
    width_total = full_rows.shape[1]
    per_sp = tp_size // 2
    column = tp_place // 2
    half = tp_place % 2
    experts_total = per_sp * sp_size
    capacity = 3 * token_count * TOP_K // (2 * experts_total)
    slot_count = sp_size * capacity
    flat_choice = route_expert.reshape(token_count * TOP_K)
    onehot = (flat_choice[:, None] == jnp.arange(experts_total, dtype=jnp.int32)[None, :]).astype(
        jnp.int32
    )
    earlier = jnp.cumsum(onehot, axis=0) - onehot
    slot_rank = jnp.sum(earlier * onehot, axis=1)
    mine = flat_choice % per_sp == column
    target = flat_choice // per_sp * capacity + slot_rank
    owner = jnp.arange(token_count * TOP_K, dtype=jnp.int32) // TOP_K
    slot_token = (
        jnp.full((slot_count + 1,), token_count, jnp.int32)
        .at[jnp.where(mine, target, slot_count)]
        .set(owner)[:slot_count]
    )
    padded = jnp.concatenate([full_rows, jnp.zeros((1, width_total), jnp.bfloat16)], axis=0)
    selected = padded[slot_token].reshape(sp_size, capacity, width_total)
    half_cap = capacity // 2
    own_part = lax.dynamic_slice_in_dim(selected, half * half_cap, half_cap, 1)
    received = core_and_chips(own_part, ("sp_0", "sp_1"), (1, 0), 0, 0)
    partner = swapped(received, "tp", 0)
    arrived = jnp.where(
        half == 0,
        jnp.concatenate([received, partner], axis=1),
        jnp.concatenate([partner, received], axis=1),
    )
    expert_rows = arrived.reshape(slot_count, width_total)
    squares = jnp.mean(jnp.square(expert_rows.astype(jnp.float32)), axis=-1, keepdims=True)
    norm_scale = lax.rsqrt(squares + EPSILON)
    gate_value = (
        jnp.dot(expert_rows, expert_gate[0], preferred_element_type=jnp.float32) * norm_scale
    )
    up_value = jnp.dot(expert_rows, expert_up[0], preferred_element_type=jnp.float32) * norm_scale
    hidden = (jax.nn.silu(gate_value) * up_value).astype(jnp.bfloat16)
    half_result = jnp.dot(hidden, expert_down[0], preferred_element_type=jnp.float32).astype(
        jnp.bfloat16
    )
    returned = core_and_chips(
        half_result.reshape(sp_size, capacity, width_total), ("sp_0", "sp_1"), (1, 0), 0, 0
    )
    slot_results = returned.reshape(slot_count, width_total)
    mine_grid = mine.reshape(token_count, TOP_K)
    target_grid = target.reshape(token_count, TOP_K)
    gathered_sum = jnp.zeros((token_count, width_total), jnp.float32)
    for choice_index in range(TOP_K):
        chosen = mine_grid[:, choice_index]
        index = jnp.where(chosen, target_grid[:, choice_index], 0)
        factor = jnp.where(chosen, route_weight[:, choice_index], 0.0)
        picked = slot_results[index].astype(jnp.float32)
        gathered_sum = gathered_sum + factor[:, None] * picked
    routed = summed_on_arrival(gathered_sum.astype(jnp.bfloat16), "tp", 1)
    return (mixed_sum + routed).astype(jnp.bfloat16)


def solution(mesh):
    split = Mesh(mesh.devices.reshape(16, 2, mesh.shape["tp"]), ("sp_0", "sp_1", "tp"))
    in_specs = (
        P(SP, "tp"),
        P(SP, "tp"),
        P(SP, "tp"),
        P("tp", None),
        P("tp", None),
        P(SP, "tp"),
        P(None, "tp"),
        P(SP, None),
        P(SP, None),
        P(SP_TP, None, None),
        P(SP_TP, None, None),
        P(SP_TP, None, None),
    )
    out_specs = P(SP, "tp")
    return jax.shard_map(local, mesh=split, in_specs=in_specs, out_specs=out_specs, check_vma=False)
```

profile of v0, /device:TPU:2, one launch (start us, length us, event | category | flops | bytes accessed | tf_op | source)
XLA Modules:
  0.0 400.2 jit_solution(6346549353143653187)
XLA Ops:
  8.5 1.4 pad_maximum_fusion
  13.3 74.1 %all-gather.2.cloned.1.call-done = bf16[8192,128]{0,1:T(8,128)(2,1)} async-done(((bf16[256,128]{0,1:T(8,128)(2,1)}), bf16[8192,128]{0,1:T(8,128)(2,1)}) %all-gather.2.cloned.1.call-update) | async-done | bytes 2097168 | tf_op jit(solution)/shard_map/all_gather | solution.py:153
  87.4 25.7 %while.18 = (s32[]{:T(128)}, f32[1,2,256]{2,1,0:T(2,128)S(1)}, f32[1,2,256]{2,1,0:T(2,128)S(1)}, f32[1,2,256,64]{2,3,1,0:T(8,128)S(1)}, bf16[8192,128]{0,1:T(8,1...) while((s32[]{:T(128)}, f32[1,2,256]{2,1,0:T(2,128)S(1)}, ...), condition=%wide.region_5.6_spmd.clone, body=%wide.region_2.5_spmd.clone.sunk | while | flops 139561984 | bytes 6914247 | solution.py:163
  89.2 1.4 fusion.75
  90.6 1.4 bitcast_reduce_fusion.3
  92.4 1.4 fusion.75
  93.8 1.4 bitcast_reduce_fusion.3
  95.6 1.4 fusion.75
  97.0 1.4 bitcast_reduce_fusion.3
  98.8 1.4 fusion.75
  102.0 1.4 fusion.75
  105.2 1.4 fusion.75
  108.5 1.4 fusion.75
  111.7 1.4 fusion.75
  114.3 7.3 %all-to-all-start = ((bf16[16,256,128]{1,2,0:T(8,128)(2,1)}), bf16[16,256,128]{1,2,0:T(8,128)(2,1)}, u32[]{:S(2)}, u32[]{:S(2)}) async-start(bf16[16,256,128]{1,2,0:T(8,128)(2,1)} %broadcast_in_dim.47), calls=%async_computation | async-start | bytes 2097152 | tf_op jit(solution)/shard_map/all_to_all | solution.py:26
  123.4 14.4 %all-to-all-done = bf16[16,256,128]{1,2,0:T(8,128)(2,1)} async-done(((bf16[16,256,128]{1,2,0:T(8,128)(2,1)}), bf16[16,256,128]{1,2,0:T(8,128)(2,1)}, u32[]{:S(2)}, u32[]{:S(2)}) %all-to-all-start) | async-done | bytes 1048608 | tf_op jit(solution)/shard_map/all_to_all | solution.py:26
  137.8 1.8 fusion.64
  140.9 5.8 %all-to-all-start.1 = ((bf16[16,256,128]{2,1,0:T(8,128)(2,1)}), bf16[16,256,128]{2,1,0:T(8,128)(2,1)}, u32[]{:S(2)}, u32[]{:S(2)}) async-start(bf16[16,256,128]{2,1,0:T(8,128)(2,1)} %broadcast_in_dim.49), calls=%async_computation.1 | async-start | bytes 2097152 | tf_op jit(solution)/shard_map/all_to_all | solution.py:26
  147.8 8.0 %scatter_custom_fusion = s32[385]{0:T(512)S(1)} fusion(s32[2048]{0:T(1024)S(1)} %bitcast.222, s32[2048]{0:T(1024)S(1)} %add_select_fusion.2, s32[]{:T(128)} %constant.176.clone.1), kind=kCustom, calls=%fused_computation.181 | custom fusion | bytes 1544 | tf_op jit(solution)/shard_map/scatter | solution.py:192
  155.8 6.1 %all-to-all-done.1 = bf16[16,256,128]{2,1,0:T(8,128)(2,1)} async-done(((bf16[16,256,128]{2,1,0:T(8,128)(2,1)}), bf16[16,256,128]{2,1,0:T(8,128)(2,1)}, u32[]{:S(2)}, u32[]{:S(2)}) %all-to-all-start.1) | async-done | bytes 1048608 | tf_op jit(solution)/shard_map/all_to_all | solution.py:26
  163.4 3.1 gather_fusion
  166.5 2.4 reshape.662
  169.8 4.4 %all_to_all.35 = bf16[16,2,1,6,2048]{4,0,3,2,1:T(8,128)(2,1)S(1)} all-to-all(bf16[16,2,1,6,2048]{4,0,3,2,1:T(8,128)(2,1)S(1)} %copy.136), channel_id=1, replica_groups=mesh['sp_0'=16,'sp_1'=2,'tp'=16] {'sp_1'}, dimensions={1} | all-to-all | bytes 1572864 | tf_op jit(solution)/shard_map/all_to_all | solution.py:43
  175.0 48.2 %all_to_all.36 = bf16[16,2,1,6,2048]{4,1,3,2,0:T(2,128)(2,1)S(1)} all-to-all(bf16[16,2,1,6,2048]{4,1,3,2,0:T(2,128)(2,1)S(1)} %copy.137), channel_id=1, replica_groups=mesh['sp_0'=16,'sp_1'=2,'tp'=16] {'sp_0'}, dimensions={0} | all-to-all | bytes 1572864 | tf_op jit(solution)/shard_map/all_to_all | solution.py:43
  224.0 3.8 collective-permute-start
  227.9 11.6 %collective-permute-done = bf16[32,6,2048]{2,0,1:T(8,128)(2,1)S(1)} collective-permute-done((bf16[32,6,2048]{2,0,1:T(8,128)(2,1)S(1)}, bf16[32,6,2048]{2,0,1:T(8,128)(2,1)S(1)}, u32[]{:S(2)}, u32[]{:S(2)}) %collective-permute-start) | collective-permute-done | bytes 786464 | tf_op jit(solution)/shard_map/ppermute | solution.py:56
  239.5 1.9 multiply_reduce_fusion
  241.6 2.3 copy.139
  245.2 2.4 convolution_multiply_fusion
  247.7 4.2 %convolution_convert_fusion = bf16[384,2048]{1,0:T(8,128)(2,1)} fusion(bf16[1,256,2048]{2,1,0:T(8,128)(2,1)S(1)} %copy-done, f32[384,256]{1,0:T(8,128)S(1)} %convolution_multiply_fusion, bf16[384,2048]{1,0:T(8,128)(2,1)S(1)} %copy-done.1, bf16[1,2048,256]{2,1,0:T(8,128)(2,1)} %param.23, f32[384]{0:T(512)S(1)} %rsqrt.30), kind=kOutput, calls=%fused_computation.32 | convolution fusion | flops 806780928 | bytes 5637632 | tf_op jit(solution)/shard_map/dot_general | solution.py:213
  251.8 2.4 reshape_reshape_reshape.6
  255.1 5.0 %all_to_all.37 = bf16[16,2,1,12,2048]{4,0,3,2,1:T(8,128)(2,1)S(1)} all-to-all(bf16[16,2,1,12,2048]{4,0,3,2,1:T(8,128)(2,1)S(1)} %copy.141), channel_id=1, replica_groups=mesh['sp_0'=16,'sp_1'=2,'tp'=16] {'sp_1'}, dimensions={1} | all-to-all | bytes 3145728 | tf_op jit(solution)/shard_map/all_to_all | solution.py:43
  260.1 2.8 copy.142
  262.9 11.4 %all-to-all-start.5 = ((bf16[16,2,1,12,2048]{4,1,3,2,0:T(2,128)(2,1)}), bf16[16,2,1,12,2048]{4,1,3,2,0:T(2,128)(2,1)S(1)}, u32[]{:S(2)}, u32[]{:S(2)}) async-start(bf16[16,2,1,12,2048]{4,1,3,2,0:T(2,128)(2,1)} %copy.142), calls=%async_computation.5 | async-start | bytes 3145728 | tf_op jit(solution)/shard_map/all_to_all | solution.py:43
  280.2 1.6 select_reduce_fusion.7
  281.8 67.1 %all-to-all-done.5 = bf16[16,2,1,12,2048]{4,1,3,2,0:T(2,128)(2,1)S(1)} async-done(((bf16[16,2,1,12,2048]{4,1,3,2,0:T(2,128)(2,1)}), bf16[16,2,1,12,2048]{4,1,3,2,0:T(2,128)(2,1)S(1)}, u32[]{:S(2)}, u32[]{:S(2)}) %all-to-all-start.5) | async-done | bytes 1572896 | tf_op jit(solution)/shard_map/all_to_all | solution.py:43
  348.9 2.1 copy.143
  351.0 2.5 reshape_reshape_reshape.7
  353.5 2.3 gather_fusion.8
  355.8 2.4 gather_fusion.7
  358.2 2.4 gather_fusion.6
  360.6 2.3 gather_fusion.5
  362.9 2.3 gather_fusion.4
  365.2 2.3 gather_fusion.3
  367.6 2.4 gather_fusion.2
  370.0 2.3 gather_fusion.1
  372.3 4.4 %fusion.26 = bf16[16,256,128]{2,1,0:T(8,128)(2,1)S(1)} fusion(f32[256]{0:T(256)S(1)} %get-tuple-element.147, f32[256]{0:T(256)S(1)} %get-tuple-element.148, f32[256]{0:T(256)S(1)} %get-tuple-element.149, f32[256]{0:T(256)S(1)} %get-tuple-element.150, f32[256]{0:T(256)S(1)} %get-tuple-element.151, f32[256]{0:T(256)S(1)} %get-tuple-element.152, ...), kind=kLoop, calls=%fused_computation.75 | loop fusion | flops 12582912 | bytes 9445376 | tf_op jit(solution)/shard_map/transpose | solution.py:36
  376.7 15.9 %all_to_all.38 = bf16[16,256,128]{2,1,0:T(8,128)(2,1)S(1)} all-to-all(bf16[16,256,128]{2,1,0:T(8,128)(2,1)S(1)} %fusion.26), channel_id=1, replica_groups=mesh['sp_0'=16,'sp_1'=2,'tp'=16] {'tp'}, dimensions={0} | all-to-all | bytes 2097152 | tf_op jit(solution)/shard_map/all_to_all | solution.py:61
  (116 shorter events, 33.5 us)
Async XLA Ops:
  6.5 241.1 %copy-start = (bf16[1,256,2048]{2,1,0:T(8,128)(2,1)S(1)}, bf16[1,256,2048]{2,1,0:T(8,128)(2,1)}, u32[]{:S(2)}) copy-start(bf16[1,256,2048]{2,1,0:T(8,128)(2,1)} %param.25) | copy-start | bytes 3145732
  6.5 80.9 %all-gather.2.cloned.1.call-start = ((), (), s32[]{:S(2)}) async-start(), calls=%async_computation.7 | async-start | bytes 2162688 | tf_op jit(solution)/shard_map/all_gather | solution.py:153
  114.3 23.6 %all-to-all-start = ((bf16[16,256,128]{1,2,0:T(8,128)(2,1)}), bf16[16,256,128]{1,2,0:T(8,128)(2,1)}, u32[]{:S(2)}, u32[]{:S(2)}) async-start(bf16[16,256,128]{1,2,0:T(8,128)(2,1)} %broadcast_in_dim.47), calls=%async_computation | async-start | bytes 2097152 | tf_op jit(solution)/shard_map/all_to_all | solution.py:26
  122.2 15.7 %copy-start.2 = (bf16[256,128]{1,0:T(8,128)(2,1)S(1)}, bf16[256,128]{1,0:T(8,128)(2,1)}, u32[]{:S(2)}) copy-start(bf16[256,128]{1,0:T(8,128)(2,1)} %param.19) | copy-start | bytes 196612
  140.9 21.0 %all-to-all-start.1 = ((bf16[16,256,128]{2,1,0:T(8,128)(2,1)}), bf16[16,256,128]{2,1,0:T(8,128)(2,1)}, u32[]{:S(2)}, u32[]{:S(2)}) async-start(bf16[16,256,128]{2,1,0:T(8,128)(2,1)} %broadcast_in_dim.49), calls=%async_computation.1 | async-start | bytes 2097152 | tf_op jit(solution)/shard_map/all_to_all | solution.py:26
  224.0 15.4 %collective-permute-start = (bf16[32,6,2048]{2,0,1:T(8,128)(2,1)S(1)}, bf16[32,6,2048]{2,0,1:T(8,128)(2,1)S(1)}, u32[]{:S(2)}, u32[]{:S(2)}) collective-permute-start(bf16[32,6,2048]{2,0,1:T(8,128)(2,1)S(1)} %reshape_reshape.7), channel_id=1, source_target_pairs={{0,1},{1,0},{2,3},{3,2},{4,5},{5,4},{6,7},{7,6},{8,9},{9,8},{10,11... | collective-permute-start | bytes 2359304 | tf_op jit(solution)/shard_map/ppermute | solution.py:56
  245.2 2.4 copy-start.1
  262.9 12.2 %copy-start.3 = (f32[256,8]{0,1:T(8,128)S(1)}, f32[256,8]{0,1:T(8,128)}, u32[]{:S(2)}) copy-start(f32[256,8]{0,1:T(8,128)} %param.22) | copy-start | bytes 24580
  262.9 86.0 %all-to-all-start.5 = ((bf16[16,2,1,12,2048]{4,1,3,2,0:T(2,128)(2,1)}), bf16[16,2,1,12,2048]{4,1,3,2,0:T(2,128)(2,1)S(1)}, u32[]{:S(2)}, u32[]{:S(2)}) async-start(bf16[16,2,1,12,2048]{4,1,3,2,0:T(2,128)(2,1)} %copy.142), calls=%async_computation.5 | async-start | bytes 3145728 | tf_op jit(solution)/shard_map/all_to_all | solution.py:43
Sparse Core Ops, SparseCore 0:
  10.1 77.2 all-gather.1
where the time goes:
time: 402 us; the launch traced here: 400 us
  waiting for transfers between devices  173 us (43%)
  blocking collectives  73.5 us (18%)
  local copies, waits for them, and re-layouts  61.2 us (15%)
  matrix products  30.6 us (8%)
  starting transfers between devices  28.4 us (7%)
  other arithmetic  19.1 us (5%)
  between operations  13.9 us (3%)
    all_gather x1, waiting for transfers between devices, local(): incoming = lax.all_gather(packed, SP, axis=0, tiled=True)  74.1 us
    all_to_all x1, waiting for transfers between devices, turned_blocks(): lax.all_to_all(pieces, axes[k], split_axis=k, concat_axis=k, tiled=True)  67.1 us
    all_to_all x3, blocking collectives, turned_blocks(): lax.all_to_all(pieces, axes[k], split_axis=k, concat_axis=k, tiled=True)  57.5 us
    all_to_all x2, waiting for transfers between devices, from_everyone(): lax.all_to_all(jnp.broadcast_to(x[None], (devices, *x.shape)), axis, 0, 0...  20.5 us
    gather x8, local copies, waits for them, and re-layouts, local(): picked = slot_results[index].astype(jnp.float32)  18.8 us
    all_to_all x1, blocking collectives, summed_on_arrival(): pieces = lax.all_to_all(cut_along(x, dim, devices), axis, 0, 0, tiled=True)  15.9 us
    all_to_all x2, starting transfers between devices, from_everyone(): lax.all_to_all(jnp.broadcast_to(x[None], (devices, *x.shape)), axis, 0, 0...  13.1 us
    ppermute x1, waiting for transfers between devices, swapped(): return lax.ppermute(value, axis, pairs)  11.6 us
  transfers between devices with their start and end apart: 5, of which 5 were waited for; matrix products, arithmetic and copies ran while one was open for 5% of the time, Pallas kernels for 0%

commit v1 on v0

--- a/solution.py
+++ b/solution.py
@@ -150,7 +150,9 @@
         jnp.zeros((local_kv, group_size, token_count), jnp.float32),
         jnp.zeros((local_kv, group_size, token_count, HEAD_DIM), jnp.float32),
     )
-    incoming = lax.all_gather(packed, SP, axis=0, tiled=True)
+    incoming = jnp.concatenate(
+        lax.all_to_all(jnp.stack([packed] * lax.axis_size(SP)), SP, 0, 0), axis=0
+    )
     incoming_len = incoming.shape[0]
     step_len = math.gcd(incoming_len, KEY_BLOCK)
 

time: 402 us -> 415 us (1.032)
  waiting for transfers between devices: 173 us -> 200 us
  starting transfers between devices: 28.4 us -> 44.8 us
  matrix products: 30.6 us -> 16.7 us
  between operations: 13.9 us -> 0.59 us
    all_to_all x0 -> x1, waiting for transfers between devices: none -> 97.2 us  [local(): lax.all_to_all(jnp.stack([packed] * lax.axis_size(SP)), SP, 0, 0)]
    all_gather x1 -> x0, waiting for transfers between devices: 74.1 us -> none  [local(): incoming = lax.all_gather(packed, SP, axis=0, tiled=True)]
    all_to_all x0 -> x1, starting transfers between devices: none -> 15.7 us  [local(): lax.all_to_all(jnp.stack([packed] * lax.axis_size(SP)), SP, 0, 0)]
    dot_general x8, matrix products: 11 us -> 3.37 us  [online_update(): jnp.einsum('tkgd,nkd->kgtn', query_groups, key_block, preferred_element_t...]
    dot_general x8, matrix products: 11.1 us -> 4.86 us  [online_update(): jnp.einsum('kgtn,nkd->kgtd', weights, value_block, preferred_element_type...]
    all_to_all x1, waiting for transfers between devices: 67.1 us -> 71.6 us  [turned_blocks(): lax.all_to_all(pieces, axes[k], split_axis=k, concat_axis=k, tiled=True)]
  transfers between devices with their start and end apart: 5 -> 5, of which waited for: 5 -> 5; matrix products, arithmetic and copies ran while one was open for 5% -> 4% of each run, Pallas kernels for 0% -> 0%
where the time goes in v1:
time: 415 us; the launch traced here: 414 us
  waiting for transfers between devices  200 us (48%)
  blocking collectives  73.6 us (18%)
  local copies, waits for them, and re-layouts  61.8 us (15%)
  starting transfers between devices  44.8 us (11%)
  matrix products  16.7 us (4%)
  other arithmetic  16.6 us (4%)
    all_to_all x1, waiting for transfers between devices, local(): lax.all_to_all(jnp.stack([packed] * lax.axis_size(SP)), SP, 0, 0)  97.2 us
    all_to_all x1, waiting for transfers between devices, turned_blocks(): lax.all_to_all(pieces, axes[k], split_axis=k, concat_axis=k, tiled=True)  71.6 us
    all_to_all x3, blocking collectives, turned_blocks(): lax.all_to_all(pieces, axes[k], split_axis=k, concat_axis=k, tiled=True)  57.4 us
    all_to_all x2, waiting for transfers between devices, from_everyone(): lax.all_to_all(jnp.broadcast_to(x[None], (devices, *x.shape)), axis, 0, 0...  19.2 us
    gather x8, local copies, waits for them, and re-layouts, local(): picked = slot_results[index].astype(jnp.float32)  18.8 us
    all_to_all x1, blocking collectives, summed_on_arrival(): pieces = lax.all_to_all(cut_along(x, dim, devices), axis, 0, 0, tiled=True)  16.2 us
    all_to_all x1, starting transfers between devices, local(): lax.all_to_all(jnp.stack([packed] * lax.axis_size(SP)), SP, 0, 0)  15.7 us
    all_to_all x2, starting transfers between devices, from_everyone(): lax.all_to_all(jnp.broadcast_to(x[None], (devices, *x.shape)), axis, 0, 0...  13.7 us
  transfers between devices with their start and end apart: 5, of which 5 were waited for; matrix products, arithmetic and copies ran while one was open for 4% of the time, Pallas kernels for 0%

profile of v1, /device:TPU:2, one launch (start us, length us, event | category | flops | bytes accessed | tf_op | source)
XLA Modules:
  0.0 414.1 jit_solution(1621782154902845675)
XLA Ops:
  0.0 0.9 fusion.46
  0.9 0.8 fusion.47
  2.8 1.5 stack.20
  4.3 15.7 %all-to-all-start = ((bf16[32,256,128]{1,2,0:T(8,128)(2,1)}), bf16[32,256,128]{1,2,0:T(8,128)(2,1)}, u32[]{:S(2)}, u32[]{:S(2)}) async-start(bf16[32,256,128]{1,2,0:T(8,128)(2,1)} %stack.20), calls=%async_computation | async-start | bytes 4194304 | tf_op jit(solution)/shard_map/all_to_all | solution.py:154
  21.8 97.2 %all-to-all-done = bf16[32,256,128]{1,2,0:T(8,128)(2,1)} async-done(((bf16[32,256,128]{1,2,0:T(8,128)(2,1)}), bf16[32,256,128]{1,2,0:T(8,128)(2,1)}, u32[]{:S(2)}, u32[]{:S(2)}) %all-to-all-start) | async-done | bytes 2097184 | tf_op jit(solution)/shard_map/all_to_all | solution.py:154
  119.0 3.2 copy.126
  122.2 11.8 %while.18 = (s32[]{:T(128)}, f32[1,2,256]{2,1,0:T(2,128)S(1)}, f32[1,2,256]{2,1,0:T(2,128)S(1)}, f32[1,2,256,64]{2,3,1,0:T(8,128)S(1)}, bf16[8192,128]{1,0:T(8,1...) while((s32[]{:T(128)}, f32[1,2,256]{2,1,0:T(2,128)S(1)}, ...), condition=%wide.region_5.6_spmd.clone, body=%wide.region_2.5_spmd.clone.sunk | while | flops 139561984 | bytes 7176391 | solution.py:165
  134.0 1.1 broadcast_in_dim.47
  135.2 7.5 %all-to-all-start.1 = ((bf16[16,256,128]{1,2,0:T(8,128)(2,1)}), bf16[16,256,128]{1,2,0:T(8,128)(2,1)}, u32[]{:S(2)}, u32[]{:S(2)}) async-start(bf16[16,256,128]{1,2,0:T(8,128)(2,1)} %broadcast_in_dim.47), calls=%async_computation.1 | async-start | bytes 2097152 | tf_op jit(solution)/shard_map/all_to_all | solution.py:26
  143.3 1.2 copy.138
  144.5 13.8 %all-to-all-done.1 = bf16[16,256,128]{1,2,0:T(8,128)(2,1)} async-done(((bf16[16,256,128]{1,2,0:T(8,128)(2,1)}), bf16[16,256,128]{1,2,0:T(8,128)(2,1)}, u32[]{:S(2)}, u32[]{:S(2)}) %all-to-all-start.1) | async-done | bytes 1048608 | tf_op jit(solution)/shard_map/all_to_all | solution.py:26
  158.3 1.8 fusion.64
  160.2 1.2 broadcast_in_dim.49
  161.4 6.2 %all-to-all-start.2 = ((bf16[16,256,128]{2,1,0:T(8,128)(2,1)}), bf16[16,256,128]{2,1,0:T(8,128)(2,1)}, u32[]{:S(2)}, u32[]{:S(2)}) async-start(bf16[16,256,128]{2,1,0:T(8,128)(2,1)} %broadcast_in_dim.49), calls=%async_computation.2 | async-start | bytes 2097152 | tf_op jit(solution)/shard_map/all_to_all | solution.py:26
  167.6 0.9 fusion.19
  168.6 8.0 %scatter_custom_fusion = s32[385]{0:T(512)S(1)} fusion(s32[2048]{0:T(1024)S(1)} %bitcast.226, s32[2048]{0:T(1024)S(1)} %add_select_fusion.2, s32[]{:T(128)} %constant.176.clone.1), kind=kCustom, calls=%fused_computation.181 | custom fusion | bytes 1544 | tf_op jit(solution)/shard_map/scatter | solution.py:194
  176.7 5.4 %all-to-all-done.2 = bf16[16,256,128]{2,1,0:T(8,128)(2,1)} async-done(((bf16[16,256,128]{2,1,0:T(8,128)(2,1)}), bf16[16,256,128]{2,1,0:T(8,128)(2,1)}, u32[]{:S(2)}, u32[]{:S(2)}) %all-to-all-start.2) | async-done | bytes 1048608 | tf_op jit(solution)/shard_map/all_to_all | solution.py:26
  182.1 1.4 copy_bitcast_fusion
  183.6 3.1 gather_fusion
  186.7 2.4 reshape.668
  189.9 4.4 %all_to_all.40 = bf16[16,2,1,6,2048]{4,0,3,2,1:T(8,128)(2,1)S(1)} all-to-all(bf16[16,2,1,6,2048]{4,0,3,2,1:T(8,128)(2,1)S(1)} %copy.140), channel_id=1, replica_groups=mesh['sp_0'=16,'sp_1'=2,'tp'=16] {'sp_1'}, dimensions={1} | all-to-all | bytes 1572864 | tf_op jit(solution)/shard_map/all_to_all | solution.py:43
  195.1 48.0 %all_to_all.41 = bf16[16,2,1,6,2048]{4,1,3,2,0:T(2,128)(2,1)S(1)} all-to-all(bf16[16,2,1,6,2048]{4,1,3,2,0:T(2,128)(2,1)S(1)} %copy.141), channel_id=1, replica_groups=mesh['sp_0'=16,'sp_1'=2,'tp'=16] {'sp_0'}, dimensions={0} | all-to-all | bytes 1572864 | tf_op jit(solution)/shard_map/all_to_all | solution.py:43
  244.0 3.9 collective-permute-start
  248.0 11.8 %collective-permute-done = bf16[32,6,2048]{2,0,1:T(8,128)(2,1)S(1)} collective-permute-done((bf16[32,6,2048]{2,0,1:T(8,128)(2,1)S(1)}, bf16[32,6,2048]{2,0,1:T(8,128)(2,1)S(1)}, u32[]{:S(2)}, u32[]{:S(2)}) %collective-permute-start) | collective-permute-done | bytes 786464 | tf_op jit(solution)/shard_map/ppermute | solution.py:56
  259.8 1.9 multiply_reduce_fusion
  261.9 2.3 copy.143
  264.2 1.3 select_n.234
  265.5 2.4 convolution_multiply_fusion
  267.9 4.2 %convolution_convert_fusion = bf16[384,2048]{1,0:T(8,128)(2,1)} fusion(bf16[1,256,2048]{2,1,0:T(8,128)(2,1)S(1)} %copy-done, f32[384,256]{1,0:T(8,128)S(1)} %convolution_multiply_fusion, bf16[384,2048]{1,0:T(8,128)(2,1)S(1)} %copy-done.2, bf16[1,2048,256]{2,1,0:T(8,128)(2,1)} %param.23, f32[384]{0:T(512)S(1)} %rsqrt.30), kind=kOutput, calls=%fused_computation.32 | convolution fusion | flops 806780928 | bytes 5637632 | tf_op jit(solution)/shard_map/dot_general | solution.py:215
  272.1 2.4 reshape_reshape_reshape.6
  274.5 0.9 copy.145
  275.4 5.0 %all_to_all.42 = bf16[16,2,1,12,2048]{4,0,3,2,1:T(8,128)(2,1)S(1)} all-to-all(bf16[16,2,1,12,2048]{4,0,3,2,1:T(8,128)(2,1)S(1)} %copy.145), channel_id=1, replica_groups=mesh['sp_0'=16,'sp_1'=2,'tp'=16] {'sp_1'}, dimensions={1} | all-to-all | bytes 3145728 | tf_op jit(solution)/shard_map/all_to_all | solution.py:43
  280.4 2.8 copy.146
  283.2 11.4 %all-to-all-start.6 = ((bf16[16,2,1,12,2048]{4,1,3,2,0:T(2,128)(2,1)}), bf16[16,2,1,12,2048]{4,1,3,2,0:T(2,128)(2,1)S(1)}, u32[]{:S(2)}, u32[]{:S(2)}) async-start(bf16[16,2,1,12,2048]{4,1,3,2,0:T(2,128)(2,1)} %copy.146), calls=%async_computation.6 | async-start | bytes 3145728 | tf_op jit(solution)/shard_map/all_to_all | solution.py:43
  296.1 0.9 fusion.36
  297.6 71.6 %all-to-all-done.6 = bf16[16,2,1,12,2048]{4,1,3,2,0:T(2,128)(2,1)S(1)} async-done(((bf16[16,2,1,12,2048]{4,1,3,2,0:T(2,128)(2,1)}), bf16[16,2,1,12,2048]{4,1,3,2,0:T(2,128)(2,1)S(1)}, u32[]{:S(2)}, u32[]{:S(2)}) %all-to-all-start.6) | async-done | bytes 1572896 | tf_op jit(solution)/shard_map/all_to_all | solution.py:43
  369.2 2.1 copy.147
  371.3 2.5 reshape_reshape_reshape.7
  373.8 2.3 gather_fusion.8
  376.1 2.4 gather_fusion.7
  378.5 2.4 gather_fusion.6
  380.9 2.3 gather_fusion.5
  383.2 2.3 gather_fusion.4
  385.5 2.3 gather_fusion.3
  387.9 2.4 gather_fusion.2
  390.3 2.3 gather_fusion.1
  392.6 4.4 %fusion.26 = bf16[16,256,128]{2,1,0:T(8,128)(2,1)S(1)} fusion(f32[256]{0:T(256)S(1)} %get-tuple-element.159, f32[256]{0:T(256)S(1)} %get-tuple-element.160, f32[256]{0:T(256)S(1)} %get-tuple-element.161, f32[256]{0:T(256)S(1)} %get-tuple-element.162, f32[256]{0:T(256)S(1)} %get-tuple-element.163, f32[256]{0:T(256)S(1)} %get-tuple-element.164, ...), kind=kLoop, calls=%fused_computation.75 | loop fusion | flops 12582912 | bytes 9445376 | tf_op jit(solution)/shard_map/transpose | solution.py:36
  397.1 16.2 %all_to_all.43 = bf16[16,256,128]{2,1,0:T(8,128)(2,1)S(1)} all-to-all(bf16[16,256,128]{2,1,0:T(8,128)(2,1)S(1)} %fusion.26), channel_id=1, replica_groups=mesh['sp_0'=16,'sp_1'=2,'tp'=16] {'tp'}, dimensions={0} | all-to-all | bytes 2097152 | tf_op jit(solution)/shard_map/all_to_all | solution.py:61
  (127 shorter events, 20.4 us)
Async XLA Ops:
  0.0 267.9 %copy-start = (bf16[1,256,2048]{2,1,0:T(8,128)(2,1)S(1)}, bf16[1,256,2048]{2,1,0:T(8,128)(2,1)}, u32[]{:S(2)}) copy-start(bf16[1,256,2048]{2,1,0:T(8,128)(2,1)} %param.25) | copy-start | bytes 3145732
  4.3 15.8 %copy-start.6 = (s32[256,8]{0,1:T(8,128)S(1)}, s32[256,8]{0,1:T(8,128)}, u32[]{:S(2)}) copy-start(s32[256,8]{0,1:T(8,128)} %param.21) | copy-start | bytes 24580
  4.3 16.9 %copy-start.8 = (f32[2,64]{1,0:T(2,128)S(1)}, f32[2,64]{1,0:T(2,128)}, u32[]{:S(2)}) copy-start(f32[2,64]{1,0:T(2,128)} %param.17) | copy-start | bytes 1540
  4.3 17.0 %copy-start.4 = (bf16[256,128]{1,0:T(8,128)(2,1)S(1)}, bf16[256,128]{1,0:T(8,128)(2,1)}, u32[]{:S(2)}) copy-start(bf16[256,128]{1,0:T(8,128)(2,1)} %param.14) | copy-start | bytes 196612
  4.3 114.7 %all-to-all-start = ((bf16[32,256,128]{1,2,0:T(8,128)(2,1)}), bf16[32,256,128]{1,2,0:T(8,128)(2,1)}, u32[]{:S(2)}, u32[]{:S(2)}) async-start(bf16[32,256,128]{1,2,0:T(8,128)(2,1)} %stack.20), calls=%async_computation | async-start | bytes 4194304 | tf_op jit(solution)/shard_map/all_to_all | solution.py:154
  135.2 23.1 %all-to-all-start.1 = ((bf16[16,256,128]{1,2,0:T(8,128)(2,1)}), bf16[16,256,128]{1,2,0:T(8,128)(2,1)}, u32[]{:S(2)}, u32[]{:S(2)}) async-start(bf16[16,256,128]{1,2,0:T(8,128)(2,1)} %broadcast_in_dim.47), calls=%async_computation.1 | async-start | bytes 2097152 | tf_op jit(solution)/shard_map/all_to_all | solution.py:26
  143.3 15.0 %copy-start.3 = (bf16[256,128]{1,0:T(8,128)(2,1)S(1)}, bf16[256,128]{1,0:T(8,128)(2,1)}, u32[]{:S(2)}) copy-start(bf16[256,128]{1,0:T(8,128)(2,1)} %param.19) | copy-start | bytes 196612
  161.4 7.1 %copy-start.5 = (s32[2048,1]{0,1:T(1,128)S(1)}, s32[2048,1]{0,1:T(1,128)}, u32[]{:S(2)}) copy-start(s32[2048,1]{0,1:T(1,128)} %reshape.666) | copy-start | bytes 24580
  161.4 20.7 %all-to-all-start.2 = ((bf16[16,256,128]{2,1,0:T(8,128)(2,1)}), bf16[16,256,128]{2,1,0:T(8,128)(2,1)}, u32[]{:S(2)}, u32[]{:S(2)}) async-start(bf16[16,256,128]{2,1,0:T(8,128)(2,1)} %broadcast_in_dim.49), calls=%async_computation.2 | async-start | bytes 2097152 | tf_op jit(solution)/shard_map/all_to_all | solution.py:26
  244.0 15.7 %collective-permute-start = (bf16[32,6,2048]{2,0,1:T(8,128)(2,1)S(1)}, bf16[32,6,2048]{2,0,1:T(8,128)(2,1)S(1)}, u32[]{:S(2)}, u32[]{:S(2)}) collective-permute-start(bf16[32,6,2048]{2,0,1:T(8,128)(2,1)S(1)} %reshape_reshape.7), channel_id=1, source_target_pairs={{0,1},{1,0},{2,3},{3,2},{4,5},{5,4},{6,7},{7,6},{8,9},{9,8},{10,11... | collective-permute-start | bytes 2359304 | tf_op jit(solution)/shard_map/ppermute | solution.py:56
  265.5 2.4 copy-start.2
  283.2 11.6 %copy-start.7 = (f32[256,8]{0,1:T(8,128)S(1)}, f32[256,8]{0,1:T(8,128)}, u32[]{:S(2)}) copy-start(f32[256,8]{0,1:T(8,128)} %param.22) | copy-start | bytes 24580
  283.2 86.0 %all-to-all-start.6 = ((bf16[16,2,1,12,2048]{4,1,3,2,0:T(2,128)(2,1)}), bf16[16,2,1,12,2048]{4,1,3,2,0:T(2,128)(2,1)S(1)}, u32[]{:S(2)}, u32[]{:S(2)}) async-start(bf16[16,2,1,12,2048]{4,1,3,2,0:T(2,128)(2,1)} %copy.146), calls=%async_computation.6 | async-start | bytes 3145728 | tf_op jit(solution)/shard_map/all_to_all | solution.py:43
  392.6 21.5 %copy-start.1 = (bf16[1,256,2048]{2,1,0:T(8,128)(2,1)S(1)}, bf16[1,256,2048]{2,1,0:T(8,128)(2,1)}, u32[]{:S(2)}) copy-start(bf16[1,256,2048]{2,1,0:T(8,128)(2,1)} %param.25) | copy-start | bytes 3145732
